TPU v7x, 32 devices: a whole 2x2x4 slice. The times are simulated.
32 devices in a mesh: ep: 8 (over z, core), tp: 4 (over y, x).
Axes of the slice: x: 2, y: 2, z: 4, core: 2. Of those that a mesh axis runs over, the one named last changes fastest.
Arguments:
- tokens: bfloat16 [1024, 2048], P('ep', 'tp')
- norm_gain: float32 [2048], P('tp'), may hold values from 0.1 to 1.9
- routing: int32 [1024, 2], P('ep'), may hold values from 0 to 3, all different within a row; in each aligned block of 128 rows (0 to 127, 128 to 255, ...) at most 80 rows name the same one
- route_weight: float32 [1024, 2], P('ep'), may hold values from 0.1 to 1
- gate_weight: bfloat16 [8, 2048, 3584], P('ep', None, 'tp'), may hold values from -0.125 to 0.125
- up_weight: bfloat16 [8, 2048, 3584], P('ep', None, 'tp'), may hold values from -0.125 to 0.125
- down_weight: bfloat16 [8, 3584, 2048], P('ep', None, 'tp')
- final_gain: float32 [2048], P('tp'), may hold values from 0.1 to 1.9
Outputs:
- mixed: bfloat16 [1024, 2048], P('ep', 'tp')
Inputs may be any that keep to these rules, and one draw needn't show every extreme that they name: `routing`: each row names 2 different experts. Among the 128 rows of one device along ep (aligned blocks), no expert is named more than 80 times, a bound that some blocks reach.
All inputs are finite; a program needn't handle non-finite values.
Results may differ from a plain program's by a relative error of at most 0.0077.
Values may be sent and summed in bfloat16 or wider, within the bound.
A program may use at most 64 MiB of HBM per device.

v0:
```python
import functools

import jax
import jax.numpy as jnp
from jax import lax
from jax.experimental import pallas as pl
from jax.experimental.pallas import tpu as pltpu
from jax.sharding import PartitionSpec as P

TOPK = 2
EPS = 1e-05
MESH = pl.DeviceIdType.MESH
F32, BF16 = jnp.float32, jnp.bfloat16


def flipped(index, mask):
    out, bit = index, 1
    while bit <= mask:
        if mask & bit:
            out = out + bit - 2 * bit * ((index // bit) % 2)
        bit *= 2
    return out


def dot(a, b):
    return jnp.dot(a, b, preferred_element_type=F32)


def dot_t(a, b):
    return lax.dot_general(a, b, (((0,), (0,)), ((), ())), preferred_element_type=F32)


def kernel(
    n, planes, groups,
    tokens, gain, routing_t, weight_t, gate_hbm, up_hbm, down_hbm, final_gain,
    out,
    wg, wu, wd, gains, picked, x, xn, hid, half_own, half_send, half_recv, pair, comb, sq_out, sq_in,
    w_sem, gain_s, gain_r, disp_s, disp_r, x_s, x_r, d2d_s, d2d_r, h_s, h_r, po_s, po_r, c_s, c_r,
    sq_s, sq_r,
):
    ep, t = lax.axis_index("ep"), lax.axis_index("tp")
    z, core = ep // 2, ep % 2
    partner = (ep + 1 - 2 * core, t)
    cap, width = picked.shape[1], picked.shape[2]
    per = planes // groups
    rows = per * cap
    inner = hid.shape[-1]
    tok_rows = tokens.shape[0]
    depth = n * width
    bits = [1 << b for b in range(n.bit_length() - 1)]
    tp_peer = [(ep, flipped(t, j)) for j in range(n)]
    tp_index = [flipped(t, j) for j in range(n)]
    expert = [flipped(z, k) for k in range(planes)]
    plane_peer = [(2 * expert[k] + core, t) for k in range(planes)]

    loads = [
        pltpu.make_async_copy(src.at[0], dst, w_sem.at[i])
        for i, (src, dst) in enumerate(((gate_hbm, wg), (up_hbm, wu), (down_hbm, wd)))
    ]
    for load in loads:
        load.start()

    barrier = pltpu.get_barrier_semaphore()
    peers = tp_peer[1:] + plane_peer[1:] + [partner]
    for peer in peers:
        pl.semaphore_signal(barrier, inc=1, device_id=peer, device_id_type=MESH)

    token_row = lax.broadcasted_iota(jnp.int32, (tok_rows, tok_rows), 0)
    token_col = lax.broadcasted_iota(jnp.int32, (tok_rows, tok_rows), 1)
    r_t0, r_t1 = routing_t[0:1, :], routing_t[1:2, :]
    wide = -(-planes // 16) * 16
    sub = lax.broadcasted_iota(jnp.int32, (wide, tok_rows), 0)
    member_t = jnp.zeros((wide, tok_rows), F32)
    for k in range(planes):
        named = ((r_t0 == expert[k]) | (r_t1 == expert[k])).astype(F32)
        member_t = jnp.where(sub == k, named, member_t)
    earlier = (token_row < token_col).astype(F32).astype(BF16)
    slot_t = dot(member_t.astype(BF16), earlier)
    slot_t = jnp.where(member_t > 0, slot_t, -1.0)
    slot_sub = lax.broadcasted_iota(jnp.int32, (cap, tok_rows), 0).astype(F32)

    def pick(k):
        chosen = (slot_sub == slot_t[k : k + 1, :]).astype(F32).astype(BF16)
        return dot(chosen, tokens[...]).astype(BF16)

    sent = []

    def remote(src, dst, s, r, peer):
        return pltpu.make_async_remote_copy(
            src_ref=src, dst_ref=dst, send_sem=s, recv_sem=r, device_id=peer, device_id_type=MESH
        )

    def start(copy):
        copy.start()
        sent.append(copy)
        return copy

    for k in range(1, planes):
        picked[k] = pick(k)
    x[0, 0, 0, 0] = pick(0)

    pl.semaphore_wait(barrier, len(peers))

    disp = [
        None if k == 0 else remote(
            picked.at[k], x.at[k // per, 0, 0, k % per], disp_s.at[k], disp_r.at[k], plane_peer[k]
        )
        for k in range(planes)
    ]
    for k in range(1, planes):
        start(disp[k])

    def tree(at, send_sem, recv_sem, order):
        copies, need = {}, {0: []}
        have = [0]
        for position, bit in enumerate(order):
            for j in list(have):
                into = j ^ bit
                copies[into] = remote(at(j), at(into), send_sem(into), recv_sem(into), tp_peer[bit])
                need[j].append(into)
                need[into] = []
                have.append(into)
        return copies, need, have[1:]

    def ascending(g):
        return bits if g % 2 == 0 else bits[::-1]

    trees = [
        tree(
            lambda j, g=g: x.at[g, j, 0], lambda j, g=g: x_s.at[g, j],
            lambda j, g=g: x_r.at[g, j], ascending(g),
        )
        for g in range(groups)
    ]
    across = [
        [remote(x.at[g, j, 0], x.at[g, j, 1], d2d_s.at[g, j], d2d_r.at[g, j], partner) for j in range(n)]
        for g in range(groups)
    ]
    hidden_trees = [
        [
            tree(
                lambda j, g=g, side=side: hid.at[g, j, side],
                lambda j, g=g, side=side: h_s.at[g, side, j],
                lambda j, g=g, side=side: h_r.at[g, side, j], ascending(side),
            )
            for side in range(2)
        ]
        for g in range(groups)
    ]

    def gather_start(g):
        for k in range(max(1, g * per), (g + 1) * per):
            disp[k].wait_recv()
        copies, need, _ = trees[g]
        for into in need[0]:
            start(copies[into])
        start(across[g][0])

    def gather_relay(g):
        copies, need, arrivals = trees[g]
        for j in arrivals:
            if need[j]:
                copies[j].wait_recv()
                for into in need[j]:
                    start(copies[into])
                start(across[g][j])

    def gather_end(g):
        copies, need, arrivals = trees[g]
        for j in arrivals:
            if not need[j]:
                copies[j].wait_recv()
                start(across[g][j])
        for j in range(n):
            across[g][j].wait_recv()

    def upward(g):
        parts = [x[g, j].reshape(2 * rows, width).astype(F32) for j in range(n)]
        square = sum(jnp.sum(p * p, axis=1, keepdims=True) for p in parts)
        scale = lax.rsqrt(square / depth + EPS)
        for j in range(n):
            columns = pl.ds(pl.multiple_of(tp_index[j] * width, width), width)
            xn[:, columns] = (parts[j] * scale * gains[j]).astype(BF16)
        for first in range(0, inner, 256):
            last = min(first + 256, inner)
            left = dot(xn[...], wg[:, first:last])
            right = dot(xn[...], wu[:, first:last])
            value = (jax.nn.silu(left) * right).astype(BF16)
            hid[g, 0, :, :, first:last] = value.reshape(2, rows, last - first)

    def hidden_start(g):
        for step in range(len(bits)):
            for side in range(2):
                copies, need, _ = hidden_trees[g][side]
                start(copies[need[0][step]])

    def hidden_relay(g):
        for side in range(2):
            copies, need, arrivals = hidden_trees[g][side]
            for j in arrivals:
                if need[j]:
                    copies[j].wait_recv()
                    for into in need[j]:
                        start(copies[into])

    halves = [
        remote(half_send.at[g], half_recv.at[g], po_s.at[g], po_r.at[g], partner) for g in range(groups)
    ]

    def downward(g):
        total = None
        for j in range(n):
            for side in range(2):
                copies, need, _ = hidden_trees[g][side]
                if j and not need[j]:
                    copies[j].wait_recv()
            part = wd[pl.ds(pl.multiple_of(tp_index[j] * inner, inner), inner), :]
            term = dot(hid[g, j].reshape(2 * rows, inner), part)
            total = term if total is None else total + term
        half_own[g] = total[:rows].astype(BF16)
        half_send[g] = total[rows:].astype(BF16)
        start(halves[g])

    back = [
        None if k == 0 else remote(
            pair.at[k // per, k % per], comb.at[k], c_s.at[k], c_r.at[k], plane_peer[k]
        )
        for k in range(planes)
    ]

    def combine(g):
        halves[g].wait_recv()
        both = (half_own[g].astype(F32) + half_recv[g].astype(F32)).astype(BF16)
        pair[g] = both.reshape(per, cap, width)
        for k in range(g * per, (g + 1) * per):
            if k == 0:
                comb[0] = both[:cap]
            else:
                start(back[k])

    gain_copies = [
        remote(gain, gains.at[j], gain_s.at[j], gain_r.at[j], tp_peer[j]) for j in range(1, n)
    ]
    gather_start(0)
    for copy in gain_copies:
        start(copy)
    gains[0] = gain[...]
    for g in range(1, groups):
        gather_start(g)
        gather_relay(g - 1)
    for copy in gain_copies:
        copy.wait_recv()
    loads[0].wait()
    loads[1].wait()
    for g in range(groups):
        gather_end(g)
        upward(g)
        if g == 0:
            gather_relay(groups - 1)
        hidden_start(g)
    loads[2].wait()
    turn = list(range(1, groups)) + [0]
    for g in turn:
        hidden_relay(g)
    for position, g in enumerate(turn):
        downward(g)
        if position:
            combine(turn[position - 1])

    w_t0, w_t1 = weight_t[0:1, :], weight_t[1:2, :]

    def share(k):
        weight = jnp.where(r_t0 == expert[k], w_t0, w_t1)
        table = jnp.where(slot_sub == slot_t[k : k + 1, :], weight, 0.0)
        high = table.astype(BF16)
        rest = table - high.astype(F32)
        middle = rest.astype(BF16)
        low = (rest - middle.astype(F32)).astype(BF16)
        block = comb[k]
        return dot_t(high, block) + (dot_t(middle, block) + dot_t(low, block))

    combine(turn[-1])
    mixed = None
    for k in list(range(1, planes)) + [0]:
        if k:
            back[k].wait_recv()
        mixed = share(k) if mixed is None else mixed + share(k)

    square = jnp.sum(mixed * mixed, axis=1, keepdims=True)
    sq_out[...] = jnp.transpose(jnp.broadcast_to(square, (tok_rows, 128)))[0:8, :]
    sums = [remote(sq_out, sq_in.at[j], sq_s.at[j], sq_r.at[j], tp_peer[j]) for j in range(1, n)]
    for copy in sums:
        start(copy)
    total = sq_out[...]
    for j in range(1, n):
        sums[j - 1].wait_recv()
        total = total + sq_in[j]
    column = jnp.transpose(jnp.broadcast_to(total[0:1, :], (128, tok_rows)))[:, 0:1]
    out[...] = (mixed * lax.rsqrt(column / depth + EPS) * final_gain[...]).astype(BF16)
    for copy in sent:
        copy.wait_send()


def shards(
    tokens, norm_gain, routing, route_weight, gate_weight, up_weight, down_weight, final_gain
):
    ep_count, n = lax.axis_size("ep"), lax.axis_size("tp")
    planes = ep_count // 2
    tok_rows, width = tokens.shape
    capacity = 2 * ((tok_rows * TOPK * 5 + planes * 8 - 1) // (planes * 8))
    cap = -(-capacity // 16) * 16
    groups = min(4, planes)
    per = planes // groups
    rows = per * cap
    depth, inner = gate_weight.shape[1:]
    dma = pltpu.SemaphoreType.DMA
    vmem, anywhere = pl.BlockSpec(memory_space=pltpu.VMEM), pl.BlockSpec(memory_space=pl.ANY)
    return pl.pallas_call(
        functools.partial(kernel, n, planes, groups),
        out_shape=jax.ShapeDtypeStruct((tok_rows, width), BF16),
        in_specs=[vmem] * 4 + [anywhere] * 3 + [vmem],
        out_specs=vmem,
        scratch_shapes=[
            pltpu.VMEM((depth, inner), BF16),
            pltpu.VMEM((depth, inner), BF16),
            pltpu.VMEM((n * inner, width), BF16),
            pltpu.VMEM((n, 1, width), F32),
            pltpu.VMEM((planes, cap, width), BF16),
            pltpu.VMEM((groups, n, 2, per, cap, width), BF16),
            pltpu.VMEM((2 * rows, depth), BF16),
            pltpu.VMEM((groups, n, 2, rows, inner), BF16),
            pltpu.VMEM((groups, rows, width), BF16),
            pltpu.VMEM((groups, rows, width), BF16),
            pltpu.VMEM((groups, rows, width), BF16),
            pltpu.VMEM((groups, per, cap, width), BF16),
            pltpu.VMEM((planes, cap, width), BF16),
            pltpu.VMEM((8, 128), F32),
            pltpu.VMEM((n, 8, 128), F32),
            dma((3,)), dma((n,)), dma((n,)), dma((planes,)), dma((planes,)),
            dma((groups, n)), dma((groups, n)), dma((groups, n)), dma((groups, n)),
            dma((groups, 2, n)), dma((groups, 2, n)), dma((groups,)), dma((groups,)),
            dma((planes,)), dma((planes,)), dma((n,)), dma((n,)),
        ],
        compiler_params=pltpu.CompilerParams(
            collective_id=0, has_side_effects=True, vmem_limit_bytes=60 * 1024 * 1024
        ),
    )(
        tokens, norm_gain.reshape(1, width), routing.T, route_weight.T,
        gate_weight, up_weight, down_weight, final_gain.reshape(1, width),
    )


def solution(mesh):
    placed = (
        P("ep", "tp"),
        P("tp"),
        P("ep", None),
        P("ep", None),
        P("ep", None, "tp"),
        P("ep", None, "tp"),
        P("ep", None, "tp"),
        P("tp"),
    )
    return jax.shard_map(
        shards, mesh=mesh, in_specs=placed, out_specs=P("ep", "tp"), check_vma=False
    )
```

profile of v0, /device:TPU:0, one launch (start us, length us, event | category | flops | bytes accessed | tf_op | source)
XLA Modules:
  0.0 72.6 jit_solution(5671073206776392725)
XLA Ops:
  0.0 71.1 %shard_map.82 = bf16[128,512]{1,0:T(8,128)(2,1)} custom-call(bf16[128,512]{1,0:T(8,128)(2,1)} %tokens.1, f32[1,512]{1,0:T(1,128)} %bitcast.4, s32[2,128]{1,0:T(2,128)} %bitcast.6, f32[2,128]{1,0:T(2,128)} %bitcast.7, bf16[1,2048,896]{2,1,0:T(8,128)(2,1)} %gate_hbm.1, bf16[1,2048,896]{2,1,0:T(8,128)(2,1)} %up_hbm.1, bf16[1,3584,512]{2,1,0:T(8,128)(2,1)} %down_hbm.1, ...), custom_call_target="tpu_custom_call" | custom-call | tf_op jit(solution)/shard_map/pallas_call | solution.py:318
  71.1 1.6 %copy.10 = bf16[128,512]{1,0:T(8,128)(2,1)} copy(bf16[128,512]{1,0:T(8,128)(2,1)} %shard_map.82) | data formatting | bytes 262144
where the time goes:
time: 72.8 us; the launch traced here: 72.6 us
  Pallas kernels  71.1 us (98%)
  local copies, waits for them, and re-layouts  1.57 us (2%)
    pallas_call x1, Pallas kernels, shards(): pl.pallas_call(functools.partial(kernel, n, planes, groups), out_shape=ja...  71.1 us
    unnamed x1, local copies, waits for them, and re-layouts  1.57 us

commit v1 on v0

--- a/solution.py
+++ b/solution.py
@@ -1,3 +1,4 @@
+import contextlib
 import functools
 
 import jax
@@ -30,18 +31,60 @@
     return lax.dot_general(a, b, (((0,), (0,)), ((), ())), preferred_element_type=F32)
 
 
+def scope(name):
+    return contextlib.nullcontext()
+
+
+def order(groups, per):
+    late = list(range(2, groups)) + [g for g in (1, 0) if g < groups]
+    steps = [("gains",), ("gs", 0), ("disp",), ("gr", 0)] if per == 1 else [
+        ("gains",), ("disp",), ("gs", 0), ("gr", 0)
+    ]
+    if groups > 1:
+        steps += [("gs", 1)]
+    steps += [("gainw",)]
+    for g in range(groups):
+        steps += [("ge", g), ("up", g)]
+        if g == 0 and groups > 1:
+            steps += [("gr", 1)]
+        if g + 2 < groups:
+            steps += [("gs", g + 2)]
+        if g and g + 1 < groups:
+            steps += [("gr", g + 1)]
+        if g == groups - 1 and g > 2:
+            steps += [("hr", g - 1)]
+        steps += [("hs", g)]
+    steps += [("wd",)]
+    relayed = [late[0]] if groups > 3 else []
+    if relayed:
+        steps += [("down", late[0])]
+    steps += [("hr", g) for g in late if g not in relayed]
+    steps += [("comb", g) for g in relayed]
+    for g in late:
+        if g not in relayed:
+            steps += [("down", g), ("comb", g)]
+    return steps
+
+
+def sequence(groups, per):
+    late = list(range(2, groups)) + [g for g in (1, 0) if g < groups]
+    return [k for g in late for k in range(g * per, (g + 1) * per) if k] + [0]
+
+
 def kernel(
     n, planes, groups,
-    tokens, gain, routing_t, weight_t, gate_hbm, up_hbm, down_hbm, final_gain,
+    tokens_hbm, gain_hbm, routing_hbm, weight_hbm, gate_hbm, up_hbm, down_hbm, final_hbm,
     out,
+    tokens, routing_t, weight_t, final_gain,
     wg, wu, wd, gains, picked, x, xn, hid, half_own, half_send, half_recv, pair, comb, sq_out, sq_in,
-    w_sem, gain_s, gain_r, disp_s, disp_r, x_s, x_r, d2d_s, d2d_r, h_s, h_r, po_s, po_r, c_s, c_r,
-    sq_s, sq_r,
+    in_sem, w_sem, gain_s, gain_r, disp_s, disp_r, x_s, x_r, d2d_s, d2d_r, h_s, h_r, po_s, po_r,
+    c_s, c_r, sq_s, sq_r,
 ):
     ep, t = lax.axis_index("ep"), lax.axis_index("tp")
     z, core = ep // 2, ep % 2
     partner = (ep + 1 - 2 * core, t)
-    cap, width = picked.shape[1], picked.shape[2]
+    pieces, cap, part = picked.shape[1:]
+    width = pieces * part
     per = planes // groups
     rows = per * cap
     inner = hid.shape[-1]
@@ -53,17 +96,26 @@
     expert = [flipped(z, k) for k in range(planes)]
     plane_peer = [(2 * expert[k] + core, t) for k in range(planes)]
 
-    loads = [
-        pltpu.make_async_copy(src.at[0], dst, w_sem.at[i])
-        for i, (src, dst) in enumerate(((gate_hbm, wg), (up_hbm, wu), (down_hbm, wd)))
-    ]
-    for load in loads:
-        load.start()
-
     barrier = pltpu.get_barrier_semaphore()
     peers = tp_peer[1:] + plane_peer[1:] + [partner]
     for peer in peers:
         pl.semaphore_signal(barrier, inc=1, device_id=peer, device_id_type=MESH)
+
+    inputs = [
+        pltpu.make_async_copy(src, dst, in_sem.at[i])
+        for i, (src, dst) in enumerate((
+            (tokens_hbm, tokens), (routing_hbm, routing_t), (gain_hbm, gains.at[0]),
+            (weight_hbm, weight_t), (final_hbm, final_gain),
+        ))
+    ]
+    loads = [
+        pltpu.make_async_copy(src.at[0], dst, w_sem.at[i])
+        for i, (src, dst) in enumerate(((gate_hbm, wg), (up_hbm, wu), (down_hbm, wd)))
+    ]
+    for load in inputs + loads:
+        load.start()
+    for load in inputs[:3]:
+        load.wait()
 
     token_row = lax.broadcasted_iota(jnp.int32, (tok_rows, tok_rows), 0)
     token_col = lax.broadcasted_iota(jnp.int32, (tok_rows, tok_rows), 1)
@@ -79,9 +131,11 @@
     slot_t = jnp.where(member_t > 0, slot_t, -1.0)
     slot_sub = lax.broadcasted_iota(jnp.int32, (cap, tok_rows), 0).astype(F32)
 
-    def pick(k):
+    def pick(k, to):
         chosen = (slot_sub == slot_t[k : k + 1, :]).astype(F32).astype(BF16)
-        return dot(chosen, tokens[...]).astype(BF16)
+        rows_of = dot(chosen, tokens[...]).astype(BF16)
+        for half in range(pieces):
+            to[half] = rows_of[:, half * part : (half + 1) * part]
 
     sent = []
 
@@ -95,21 +149,19 @@
         sent.append(copy)
         return copy
 
+    pick(0, x.at[0, 0, 0, :, 0])
     for k in range(1, planes):
-        picked[k] = pick(k)
-    x[0, 0, 0, 0] = pick(0)
-
-    pl.semaphore_wait(barrier, len(peers))
+        pick(k, picked.at[k])
+
+    with scope("barrier"):
+        pl.semaphore_wait(barrier, len(peers))
 
     disp = [
         None if k == 0 else remote(
-            picked.at[k], x.at[k // per, 0, 0, k % per], disp_s.at[k], disp_r.at[k], plane_peer[k]
+            picked.at[k], x.at[k // per, 0, 0, :, k % per], disp_s.at[k], disp_r.at[k], plane_peer[k]
         )
         for k in range(planes)
     ]
-    for k in range(1, planes):
-        start(disp[k])
-
     def tree(at, send_sem, recv_sem, order):
         copies, need = {}, {0: []}
         have = [0]
@@ -126,14 +178,27 @@
         return bits if g % 2 == 0 else bits[::-1]
 
     trees = [
-        tree(
-            lambda j, g=g: x.at[g, j, 0], lambda j, g=g: x_s.at[g, j],
-            lambda j, g=g: x_r.at[g, j], ascending(g),
-        )
+        [
+            tree(
+                lambda j, g=g, half=half: x.at[g, j, 0, half],
+                lambda j, g=g, half=half: x_s.at[g, half, j],
+                lambda j, g=g, half=half: x_r.at[g, half, j], ascending(half if pieces > 1 else g),
+            )
+            for half in range(pieces)
+        ]
         for g in range(groups)
     ]
     across = [
-        [remote(x.at[g, j, 0], x.at[g, j, 1], d2d_s.at[g, j], d2d_r.at[g, j], partner) for j in range(n)]
+        [
+            [
+                remote(
+                    x.at[g, j, 0, half], x.at[g, j, 1, half],
+                    d2d_s.at[g, half, j], d2d_r.at[g, half, j], partner,
+                )
+                for j in range(n)
+            ]
+            for half in range(pieces)
+        ]
         for g in range(groups)
     ]
     hidden_trees = [
@@ -151,36 +216,46 @@
     def gather_start(g):
         for k in range(max(1, g * per), (g + 1) * per):
             disp[k].wait_recv()
-        copies, need, _ = trees[g]
-        for into in need[0]:
-            start(copies[into])
-        start(across[g][0])
+        for step in range(len(bits)):
+            for half in range(pieces):
+                copies, need, _ = trees[g][half]
+                start(copies[need[0][step]])
+        for half in range(pieces):
+            start(across[g][half][0])
 
     def gather_relay(g):
-        copies, need, arrivals = trees[g]
-        for j in arrivals:
-            if need[j]:
-                copies[j].wait_recv()
-                for into in need[j]:
-                    start(copies[into])
-                start(across[g][j])
+        for half in range(pieces):
+            copies, need, arrivals = trees[g][half]
+            for j in arrivals:
+                if need[j]:
+                    copies[j].wait_recv()
+                    for into in need[j]:
+                        start(copies[into])
+                    start(across[g][half][j])
 
     def gather_end(g):
-        copies, need, arrivals = trees[g]
-        for j in arrivals:
-            if not need[j]:
-                copies[j].wait_recv()
-                start(across[g][j])
-        for j in range(n):
-            across[g][j].wait_recv()
+        for last in range(2):
+            for half in range(pieces):
+                copies, need, arrivals = trees[g][half]
+                for j in arrivals:
+                    if not need[j] and (j == n - 1) == bool(last):
+                        copies[j].wait_recv()
+                        start(across[g][half][j])
+        for half in range(pieces):
+            for j in range(n):
+                across[g][half][j].wait_recv()
 
     def upward(g):
-        parts = [x[g, j].reshape(2 * rows, width).astype(F32) for j in range(n)]
-        square = sum(jnp.sum(p * p, axis=1, keepdims=True) for p in parts)
+        blocks = [
+            [x[g, j, :, half].reshape(2 * rows, part).astype(F32) for half in range(pieces)] for j in range(n)
+        ]
+        square = sum(jnp.sum(p * p, axis=1, keepdims=True) for of_peer in blocks for p in of_peer)
         scale = lax.rsqrt(square / depth + EPS)
         for j in range(n):
-            columns = pl.ds(pl.multiple_of(tp_index[j] * width, width), width)
-            xn[:, columns] = (parts[j] * scale * gains[j]).astype(BF16)
+            for half in range(pieces):
+                columns = pl.ds(pl.multiple_of(tp_index[j] * width + half * part, part), part)
+                own = gains[j, :, half * part : (half + 1) * part]
+                xn[:, columns] = (blocks[j][half] * scale * own).astype(BF16)
         for first in range(0, inner, 256):
             last = min(first + 256, inner)
             left = dot(xn[...], wg[:, first:last])
@@ -239,33 +314,36 @@
                 start(back[k])
 
     gain_copies = [
-        remote(gain, gains.at[j], gain_s.at[j], gain_r.at[j], tp_peer[j]) for j in range(1, n)
-    ]
-    gather_start(0)
-    for copy in gain_copies:
-        start(copy)
-    gains[0] = gain[...]
-    for g in range(1, groups):
-        gather_start(g)
-        gather_relay(g - 1)
-    for copy in gain_copies:
-        copy.wait_recv()
-    loads[0].wait()
-    loads[1].wait()
-    for g in range(groups):
-        gather_end(g)
-        upward(g)
-        if g == 0:
-            gather_relay(groups - 1)
-        hidden_start(g)
-    loads[2].wait()
-    turn = list(range(1, groups)) + [0]
-    for g in turn:
-        hidden_relay(g)
-    for position, g in enumerate(turn):
-        downward(g)
-        if position:
-            combine(turn[position - 1])
+        remote(gains.at[0], gains.at[j], gain_s.at[j], gain_r.at[j], tp_peer[j]) for j in range(1, n)
+    ]
+
+    def dispatch():
+        for k in range(1, planes):
+            start(disp[k])
+
+    def gains_start():
+        for copy in gain_copies:
+            start(copy)
+
+    def gains_end():
+        for copy in gain_copies:
+            copy.wait_recv()
+        for load in inputs[3:]:
+            load.wait()
+        loads[0].wait()
+        loads[1].wait()
+
+    def run(steps):
+        for name, *of in steps:
+            with scope(name + "".join(str(g) for g in of)):
+                actions[name](*of)
+
+    actions = dict(
+        disp=dispatch, gs=gather_start, gr=gather_relay, ge=gather_end, up=upward, hs=hidden_start,
+        hr=hidden_relay, gains=gains_start, gainw=gains_end, wd=lambda: loads[2].wait(),
+        down=downward, comb=combine,
+    )
+    run(order(groups, per))
 
     w_t0, w_t1 = weight_t[0:1, :], weight_t[1:2, :]
 
@@ -279,12 +357,12 @@
         block = comb[k]
         return dot_t(high, block) + (dot_t(middle, block) + dot_t(low, block))
 
-    combine(turn[-1])
     mixed = None
-    for k in list(range(1, planes)) + [0]:
-        if k:
-            back[k].wait_recv()
-        mixed = share(k) if mixed is None else mixed + share(k)
+    for k in sequence(groups, per):
+        with scope(f"share{k}"):
+            if k:
+                back[k].wait_recv()
+            mixed = share(k) if mixed is None else mixed + share(k)
 
     square = jnp.sum(mixed * mixed, axis=1, keepdims=True)
     sq_out[...] = jnp.transpose(jnp.broadcast_to(square, (tok_rows, 128)))[0:8, :]
@@ -292,13 +370,15 @@
     for copy in sums:
         start(copy)
     total = sq_out[...]
-    for j in range(1, n):
-        sums[j - 1].wait_recv()
-        total = total + sq_in[j]
+    with scope("sqwait"):
+        for j in range(1, n):
+            sums[j - 1].wait_recv()
+            total = total + sq_in[j]
     column = jnp.transpose(jnp.broadcast_to(total[0:1, :], (128, tok_rows)))[:, 0:1]
     out[...] = (mixed * lax.rsqrt(column / depth + EPS) * final_gain[...]).astype(BF16)
-    for copy in sent:
-        copy.wait_send()
+    with scope("wsend"):
+        for copy in sent:
+            copy.wait_send()
 
 
 def shards(
@@ -312,21 +392,27 @@
     groups = min(4, planes)
     per = planes // groups
     rows = per * cap
+    pieces = 2 if width % 256 == 0 else 1
+    part = width // pieces
     depth, inner = gate_weight.shape[1:]
     dma = pltpu.SemaphoreType.DMA
     vmem, anywhere = pl.BlockSpec(memory_space=pltpu.VMEM), pl.BlockSpec(memory_space=pl.ANY)
     return pl.pallas_call(
         functools.partial(kernel, n, planes, groups),
-        out_shape=jax.ShapeDtypeStruct((tok_rows, width), BF16),
-        in_specs=[vmem] * 4 + [anywhere] * 3 + [vmem],
+        out_shape=pltpu.VMEM((tok_rows, width), BF16),
+        in_specs=[anywhere] * 8,
         out_specs=vmem,
         scratch_shapes=[
+            pltpu.VMEM((tok_rows, width), BF16),
+            pltpu.VMEM((TOPK, tok_rows), jnp.int32),
+            pltpu.VMEM((TOPK, tok_rows), F32),
+            pltpu.VMEM((1, width), F32),
             pltpu.VMEM((depth, inner), BF16),
             pltpu.VMEM((depth, inner), BF16),
             pltpu.VMEM((n * inner, width), BF16),
             pltpu.VMEM((n, 1, width), F32),
-            pltpu.VMEM((planes, cap, width), BF16),
-            pltpu.VMEM((groups, n, 2, per, cap, width), BF16),
+            pltpu.VMEM((planes, pieces, cap, part), BF16),
+            pltpu.VMEM((groups, n, 2, pieces, per, cap, part), BF16),
             pltpu.VMEM((2 * rows, depth), BF16),
             pltpu.VMEM((groups, n, 2, rows, inner), BF16),
             pltpu.VMEM((groups, rows, width), BF16),
@@ -336,8 +422,8 @@
             pltpu.VMEM((planes, cap, width), BF16),
             pltpu.VMEM((8, 128), F32),
             pltpu.VMEM((n, 8, 128), F32),
-            dma((3,)), dma((n,)), dma((n,)), dma((planes,)), dma((planes,)),
-            dma((groups, n)), dma((groups, n)), dma((groups, n)), dma((groups, n)),
+            dma((5,)), dma((3,)), dma((n,)), dma((n,)), dma((planes,)), dma((planes,)),
+            dma((groups, pieces, n)), dma((groups, pieces, n)), dma((groups, pieces, n)), dma((groups, pieces, n)),
             dma((groups, 2, n)), dma((groups, 2, n)), dma((groups,)), dma((groups,)),
             dma((planes,)), dma((planes,)), dma((n,)), dma((n,)),
         ],

time: 72.8 us -> 68 us (0.934)
  Pallas kernels: 71.1 us -> 67.2 us
  local copies, waits for them, and re-layouts: 1.57 us -> 0.66 us
    pallas_call x1, Pallas kernels: 71.1 us -> 67.2 us  [shards(): pl.pallas_call(functools.partial(kernel, n, planes, groups), out_shape=pl...]
    unnamed x1, local copies, waits for them, and re-layouts: 1.57 us -> 0.66 us
where the time goes in v1:
time: 68 us; the launch traced here: 67.8 us
  Pallas kernels  67.2 us (99%)
    pallas_call x1, Pallas kernels, shards(): pl.pallas_call(functools.partial(kernel, n, planes, groups), out_shape=pl...  67.2 us

profile of v1, /device:TPU:0, one launch (start us, length us, event | category | flops | bytes accessed | tf_op | source)
XLA Modules:
  0.0 67.8 jit_solution(13802953391509966070)
XLA Ops:
  0.0 67.2 %shard_map.82 = bf16[128,512]{1,0:T(8,128)(2,1)S(1)} custom-call(bf16[128,512]{1,0:T(8,128)(2,1)} %tokens_hbm.1, f32[1,512]{1,0:T(1,128)} %bitcast.4, s32[2,128]{1,0:T(2,128)} %bitcast.6, f32[2,128]{1,0:T(2,128)} %bitcast.7, bf16[1,2048,896]{2,1,0:T(8,128)(2,1)} %gate_hbm.1, bf16[1,2048,896]{2,1,0:T(8,128)(2,1)} %up_hbm.1, bf16[1,3584,512]{2,1,0:T(8,128)(2,1)} %down_hbm.1, ...), custom_call_target="tpu_custom_call" | custom-call | tf_op jit(solution)/shard_map/pallas_call | solution.py:400
  67.2 0.7 copy.10

commit v2 on v1

v2 whole, which is shorter than its diff:
```python
import contextlib
import functools

import jax
import jax.numpy as jnp
from jax import lax
from jax.experimental import pallas as pl
from jax.experimental.pallas import tpu as pltpu
from jax.sharding import PartitionSpec as P

TOPK = 2
EPS = 1e-05
MESH = pl.DeviceIdType.MESH
F32, BF16 = jnp.float32, jnp.bfloat16


def scope(name):
    return contextlib.nullcontext()


def flipped(index, mask):
    out, bit = index, 1
    while bit <= mask:
        if mask & bit:
            out = out + bit - 2 * bit * ((index // bit) % 2)
        bit *= 2
    return out


def dot(a, b):
    return jnp.dot(a, b, preferred_element_type=F32)


def dot_t(a, b):
    return lax.dot_general(a, b, (((0,), (0,)), ((), ())), preferred_element_type=F32)


def spread(n, backwards):
    bits = [1 << b for b in range(n.bit_length() - 1)]
    edges, need, have = [], {0: []}, [0]
    for bit in bits[::-1] if backwards else bits:
        for j in list(have):
            edges.append((j, j ^ bit, bit))
            need[j].append(j ^ bit)
            need[j ^ bit] = []
            have.append(j ^ bit)
    return edges, need, have[1:]


def arrivals(n, ways):
    slots, count = {}, 0
    trees = [spread(n, backwards) for backwards in ways]
    for j in range(1, n):
        alone = any(need[j] for _, need, _ in trees)
        for i in range(len(ways)):
            slots[i, j] = count
            count += alone
        count += not alone
    return slots, count


def wide_groups(planes, per):
    return (1, 2) if per == 1 and planes == 4 else ()


def ways_of(pieces, g):
    return [bool(i % 2) for i in range(pieces)] if pieces > 1 else [bool(g % 2)]


def order(groups, per, wide):
    if wide:
        return [
            ("first",), ("trelay",), ("tend",), ("gs", 3), ("loaded",), ("xs", 0), ("up", 0), ("gr", 3), ("hs", 0),
            ("ge", 3), ("xs", 3), ("up", 3), ("hs", 3), ("xw", 1), ("xs", 1), ("up", 1), ("hs", 1), ("hr", 3),
            ("xw", 2), ("xs", 2), ("up", 2), ("hs", 2), ("down", 3), ("comb", 3), ("hr", 2), ("hr", 1), ("hr", 0),
            ("down", 2), ("comb", 2), ("down", 1), ("comb", 1), ("down", 0), ("comb", 0),
        ]
    late = list(range(2, groups)) + [g for g in (1, 0) if g < groups]
    steps = [("first",), ("gs", 0), ("gr", 0)]
    if groups > 1:
        steps += [("gs", 1)]
    steps += [("loaded",)]
    for g in range(groups):
        steps += [("ge", g), ("xs", g), ("up", g)]
        if g == 0 and groups > 1:
            steps += [("gr", 1)]
        if g + 2 < groups:
            steps += [("gs", g + 2)]
        if g and g + 1 < groups:
            steps += [("gr", g + 1)]
        if g == groups - 1 and g > 2:
            steps += [("hr", g - 1)]
        steps += [("hs", g)]
    relayed = [late[0]] if groups > 3 else []
    steps += [("down", g) for g in relayed]
    steps += [("hr", g) for g in late if g not in relayed]
    steps += [("comb", g) for g in relayed]
    for g in late:
        if g not in relayed:
            steps += [("down", g), ("comb", g)]
    return steps


def returned(steps, per):
    late = [of[0] for name, *of in steps if name == "comb"]
    return [k for g in late for k in range(g * per, (g + 1) * per) if k] + [0]


def kernel(
    n, planes, groups, wide,
    tokens_hbm, gain_hbm, routing_hbm, weight_hbm, gate_hbm, up_hbm, down_hbm, final_hbm,
    out,
    tokens, routing_t, weight_t, final_gain,
    wg, wu, wd, gains, picked, chosen_wide, x, xn, hid, half_own, half_send, half_recv, pair, comb, sq_out, sq_in,
    in_sem, w_sem, out_sem, gain_r, tok_r, disp_r, wide_r, x_r, d2d_r, h_r, po_r, c_r, sq_r,
):
    ep, t = lax.axis_index("ep"), lax.axis_index("tp")
    z, core = ep // 2, ep % 2
    partner = (ep + 1 - 2 * core, t)
    pieces, cap, part = picked.shape[1:]
    width = pieces * part
    per = planes // groups
    rows = per * cap
    inner = hid.shape[-1]
    tok_rows = tokens.shape[1]
    depth = n * width
    tp_peer = [(ep, flipped(t, j)) for j in range(n)]
    tp_index = [flipped(t, j) for j in range(n)]
    expert = [flipped(z, k) for k in range(planes)]
    plane_peer = [(2 * expert[k] + core, t) for k in range(planes)]
    narrow = [k for k in range(1, planes) if k // per not in wide]
    gathered = [g for g in range(groups) if not wide or (g and g not in wide)]

    barrier = pltpu.get_barrier_semaphore()
    peers = tp_peer[1:] + plane_peer[1:] + [partner]
    for peer in peers:
        pl.semaphore_signal(barrier, inc=1, device_id=peer, device_id_type=MESH)

    inputs = [
        pltpu.make_async_copy(src, dst, in_sem.at[i])
        for i, (src, dst) in enumerate((
            (tokens_hbm, tokens.at[0]), (routing_hbm, routing_t), (gain_hbm, gains.at[0]),
            (weight_hbm, weight_t), (final_hbm, final_gain),
        ))
    ]
    loads = [
        pltpu.make_async_copy(src.at[0], dst, w_sem.at[i])
        for i, (src, dst) in enumerate(((gate_hbm, wg), (up_hbm, wu), (down_hbm, wd)))
    ]
    for load in inputs + loads:
        load.start()
    for load in inputs[:3]:
        load.wait()

    token_row = lax.broadcasted_iota(jnp.int32, (tok_rows, tok_rows), 0)
    token_col = lax.broadcasted_iota(jnp.int32, (tok_rows, tok_rows), 1)
    r_t0, r_t1 = routing_t[0:1, :], routing_t[1:2, :]
    tall = -(-planes // 16) * 16
    sub = lax.broadcasted_iota(jnp.int32, (tall, tok_rows), 0)
    member_t = jnp.zeros((tall, tok_rows), F32)
    for k in range(planes):
        named = ((r_t0 == expert[k]) | (r_t1 == expert[k])).astype(F32)
        member_t = jnp.where(sub == k, named, member_t)
    earlier = (token_row < token_col).astype(F32).astype(BF16)
    slot_t = dot(member_t.astype(BF16), earlier)
    slot_t = jnp.where(member_t > 0, slot_t, -1.0)
    slot_sub = lax.broadcasted_iota(jnp.int32, (cap, tok_rows), 0).astype(F32)

    def pick(k, j, to):
        chosen = (slot_sub == slot_t[k : k + 1, :]).astype(F32).astype(BF16)
        found = dot(chosen, tokens[j]).astype(BF16)
        for i in range(pieces):
            to[i] = found[:, i * part : (i + 1) * part]

    def remote(src, dst, s, r, peer):
        return pltpu.make_async_remote_copy(
            src_ref=src, dst_ref=dst, send_sem=s, recv_sem=r, device_id=peer, device_id_type=MESH
        )

    sent = {}

    def start(copy, sem, ref):
        copy.start()
        sent[sem] = ref
        return copy

    class Cast:
        def __init__(self, at, whole, ways, sem, total, slot):
            self.at, self.whole, self.sem, self.total, self.slot = at, whole, sem, total, slot
            self.trees = [spread(n, backwards) for backwards in ways]
            self.slots = arrivals(n, ways)[0]
            self.copies = [
                {
                    into: remote(at(i, j), at(i, into), out_sem.at[sem], slot(self.slots[i, into]), tp_peer[bit])
                    for j, into, bit in edges
                }
                for i, (edges, _, _) in enumerate(self.trees)
            ]

        def begin(self):
            for step in range(n.bit_length() - 1):
                for i, (_, need, _) in enumerate(self.trees):
                    start(self.copies[i][need[0][step]], self.sem, self.total)

        def relay(self, then=None):
            for i, (_, need, come) in enumerate(self.trees):
                for j in come:
                    if need[j]:
                        self.copies[i][j].wait_recv()
                        for into in need[j]:
                            start(self.copies[i][into], self.sem, self.total)
                        if then:
                            then(i, j)

        def settle(self, j, then=None, then_all=None):
            ends = [i for i, (_, need, _) in enumerate(self.trees) if not need[j]]
            if len(ends) == len(self.trees):
                ref = self.whole(j)
                remote(ref, ref, out_sem.at[self.sem], self.slot(self.slots[0, j]), tp_peer[j]).wait_recv()
                if then_all:
                    then_all(j)
                return
            for i in ends:
                self.copies[i][j].wait_recv()
                if then:
                    then(i, j)

    TOK, DISP, WIDE, X, D2D, H, PO, C, SQ, GAIN = range(10)

    with scope("picks"):
        pick(0, 0, x.at[0, 0, 0, :, 0])
        for at, k in enumerate(narrow):
            pick(k, 0, picked.at[at])
        for at, k in enumerate(wide):
            pick(k, 0, chosen_wide.at[at, 0])

    with scope("barrier"):
        pl.semaphore_wait(barrier, len(peers))

    disp = {
        k: remote(
            picked.at[at], x.at[k // per, 0, 0, :, k % per], out_sem.at[DISP], disp_r.at[at], plane_peer[k]
        )
        for at, k in enumerate(narrow)
    }

    def across(g, j):
        start(
            remote(x.at[g, j, 0], x.at[g, j, 1], out_sem.at[D2D], d2d_r.at[g], partner), D2D, x.at[:, :, 0]
        )

    def across_piece(g):
        return lambda i, j: start(
            remote(x.at[g, j, 0, i], x.at[g, j, 1, i], out_sem.at[D2D], d2d_r.at[g], partner), D2D, x.at[:, :, 0]
        )

    def across_end(g):
        ref = x.at[g, :, 1]
        remote(ref, ref, out_sem.at[D2D], d2d_r.at[g], partner).wait_recv()

    def wide_copy(at, j):
        k = wide[at]
        return remote(
            chosen_wide.at[at, j], x.at[k, j, 0, :, 0], out_sem.at[WIDE], wide_r.at[at, j], plane_peer[k]
        )

    if wide:
        quarters = len(ways_of_tokens(tok_rows))
        tall_piece = tok_rows // quarters
        token_cast = Cast(
            lambda i, j: tokens.at[j, i * tall_piece : (i + 1) * tall_piece], lambda j: tokens.at[j],
            ways_of_tokens(tok_rows), TOK, tokens.at[0 : n - 1], lambda slot: tok_r.at[slot],
        )
    x_casts = {
        g: Cast(
            lambda i, j, g=g: x.at[g, j, 0, i], lambda j, g=g: x.at[g, j, 0],
            ways_of(pieces, g), X, x.at[gathered[0] :, 0 : n - 1, 0],
            lambda slot, at=at: x_r.at[at, slot],
        )
        for at, g in enumerate(gathered)
    }
    h_casts = [
        Cast(
            lambda i, j, g=g: hid.at[g, j, i], lambda j, g=g: hid.at[g, j],
            [False, True], H, hid.at[:, 0 : n - 1], lambda slot, g=g: h_r.at[g, slot],
        )
        for g in range(groups)
    ]
    gain_copies = [
        remote(gains.at[0], gains.at[j], out_sem.at[GAIN], gain_r.at[0], tp_peer[j]) for j in range(1, n)
    ]

    def first():
        if wide:
            token_cast.begin()
            across(0, 0)
        for copy in gain_copies:
            start(copy, GAIN, gains.at[1:])
        for k in narrow:
            start(disp[k], DISP, picked)
        for at in range(len(wide)):
            start(wide_copy(at, 0), WIDE, chosen_wide)

    def tokens_end():
        for j in range(1, n):
            token_cast.settle(j)
            pick(0, j, x.at[0, j, 0, :, 0])
            across(0, j)
            for at, k in enumerate(wide):
                pick(k, j, chosen_wide.at[at, j])
                start(wide_copy(at, j), WIDE, chosen_wide)

    def wide_end(g):
        for j in range(n):
            wide_copy(wide.index(g), j).wait_recv()
            across(g, j)

    def gather_start(g):
        for k in range(max(1, g * per), (g + 1) * per):
            disp[k].wait_recv()
        x_casts[g].begin()
        across(g, 0)

    def gather_end(g):
        for j in range(1, n):
            x_casts[g].settle(j, across_piece(g), lambda j: across(g, j))

    def loaded():
        remote(gains.at[1:], gains.at[1:], out_sem.at[GAIN], gain_r.at[0], partner).wait_recv()
        for load in inputs[3:] + loads:
            load.wait()

    def upward(g):
        blocks = [
            [x[g, j, :, i].reshape(2 * rows, part).astype(F32) for i in range(pieces)] for j in range(n)
        ]
        square = sum(jnp.sum(p * p, axis=1, keepdims=True) for of_peer in blocks for p in of_peer)
        scale = lax.rsqrt(square / depth + EPS)
        for j in range(n):
            for i in range(pieces):
                columns = pl.ds(pl.multiple_of(tp_index[j] * width + i * part, part), part)
                own = gains[j, :, i * part : (i + 1) * part]
                xn[:, columns] = (blocks[j][i] * scale * own).astype(BF16)
        for first in range(0, inner, 256):
            last = min(first + 256, inner)
            left = dot(xn[...], wg[:, first:last])
            right = dot(xn[...], wu[:, first:last])
            value = (jax.nn.silu(left) * right).astype(BF16)
            hid[g, 0, :, :, first:last] = value.reshape(2, rows, last - first)

    halves = [
        remote(half_send.at[g], half_recv.at[g], out_sem.at[PO], po_r.at[g], partner) for g in range(groups)
    ]

    def downward(g):
        total = None
        for j in range(n):
            if j:
                h_casts[g].settle(j)
            block = wd[pl.ds(pl.multiple_of(tp_index[j] * inner, inner), inner), :]
            term = dot(hid[g, j].reshape(2 * rows, inner), block)
            total = term if total is None else total + term
        half_own[g] = total[:rows].astype(BF16)
        half_send[g] = total[rows:].astype(BF16)
        start(halves[g], PO, half_send)

    back = {
        k: remote(pair.at[k // per, k % per], comb.at[k], out_sem.at[C], c_r.at[k - 1], plane_peer[k])
        for k in range(1, planes)
    }

    def combine(g):
        halves[g].wait_recv()
        both = (half_own[g].astype(F32) + half_recv[g].astype(F32)).astype(BF16)
        pair[g] = both.reshape(per, cap, width)
        for k in range(g * per, (g + 1) * per):
            if k == 0:
                comb[0] = both[:cap]
            else:
                start(back[k], C, comb.at[1:])

    actions = dict(
        first=first, tend=tokens_end, gs=gather_start, ge=gather_end, xs=across_end, xw=wide_end, up=upward,
        loaded=loaded, hs=lambda g: h_casts[g].begin(), hr=lambda g: h_casts[g].relay(), down=downward,
        comb=combine, gr=lambda g: x_casts[g].relay(across_piece(g)), trelay=lambda: token_cast.relay(),
    )
    steps = order(groups, per, wide)
    for name, *of in steps:
        with scope(name + "".join(str(g) for g in of)):
            actions[name](*of)

    w_t0, w_t1 = weight_t[0:1, :], weight_t[1:2, :]

    def share(k):
        weight = jnp.where(r_t0 == expert[k], w_t0, w_t1)
        table = jnp.where(slot_sub == slot_t[k : k + 1, :], weight, 0.0)
        high = table.astype(BF16)
        rest = table - high.astype(F32)
        middle = rest.astype(BF16)
        low = (rest - middle.astype(F32)).astype(BF16)
        block = comb[k]
        return dot_t(high, block) + (dot_t(middle, block) + dot_t(low, block))

    mixed = None
    for k in returned(steps, per):
        with scope(f"share{k}"):
            if k:
                back[k].wait_recv()
            mixed = share(k) if mixed is None else mixed + share(k)

    square = jnp.sum(mixed * mixed, axis=1, keepdims=True)
    sq_out[...] = jnp.transpose(jnp.broadcast_to(square, (tok_rows, 128)))[0:8, :]
    for j in range(1, n):
        start(remote(sq_out, sq_in.at[j], out_sem.at[SQ], sq_r.at[0], tp_peer[j]), SQ, sq_in.at[1:])
    with scope("sqwait"):
        remote(sq_in.at[1:], sq_in.at[1:], out_sem.at[SQ], sq_r.at[0], partner).wait_recv()
    total = sq_out[...]
    for j in range(1, n):
        total = total + sq_in[j]
    column = jnp.transpose(jnp.broadcast_to(total[0:1, :], (128, tok_rows)))[:, 0:1]
    out[...] = (mixed * lax.rsqrt(column / depth + EPS) * final_gain[...]).astype(BF16)
    with scope("wsend"):
        for sem, ref in sent.items():
            remote(ref, ref, out_sem.at[sem], sq_r.at[0], partner).wait_send()


def ways_of_tokens(tok_rows):
    return [False, True] * (2 if tok_rows % 64 == 0 else 1)


def shards(
    tokens, norm_gain, routing, route_weight, gate_weight, up_weight, down_weight, final_gain
):
    ep_count, n = lax.axis_size("ep"), lax.axis_size("tp")
    planes = ep_count // 2
    tok_rows, width = tokens.shape
    capacity = 2 * ((tok_rows * TOPK * 5 + planes * 8 - 1) // (planes * 8))
    cap = -(-capacity // 16) * 16
    groups = min(4, planes)
    per = planes // groups
    rows = per * cap
    wide = wide_groups(planes, per)
    pieces = 2 if width % 256 == 0 else 1
    part = width // pieces
    depth, inner = gate_weight.shape[1:]
    few = max(1, len(wide))
    gathered = groups - 1 - len(wide) if wide else groups
    narrow = planes - 1 - len(wide)
    dma = pltpu.SemaphoreType.DMA
    vmem, anywhere = pl.BlockSpec(memory_space=pltpu.VMEM), pl.BlockSpec(memory_space=pl.ANY)
    return pl.pallas_call(
        functools.partial(kernel, n, planes, groups, wide),
        out_shape=pltpu.VMEM((tok_rows, width), BF16),
        in_specs=[anywhere] * 8,
        out_specs=vmem,
        scratch_shapes=[
            pltpu.VMEM((n if wide else 1, tok_rows, width), BF16),
            pltpu.VMEM((TOPK, tok_rows), jnp.int32),
            pltpu.VMEM((TOPK, tok_rows), F32),
            pltpu.VMEM((1, width), F32),
            pltpu.VMEM((depth, inner), BF16),
            pltpu.VMEM((depth, inner), BF16),
            pltpu.VMEM((n * inner, width), BF16),
            pltpu.VMEM((n, 1, width), F32),
            pltpu.VMEM((max(1, narrow), pieces, cap, part), BF16),
            pltpu.VMEM((few, n if wide else 1, pieces, cap, part), BF16),
            pltpu.VMEM((groups, n, 2, pieces, per, cap, part), BF16),
            pltpu.VMEM((2 * rows, depth), BF16),
            pltpu.VMEM((groups, n, 2, rows, inner), BF16),
            pltpu.VMEM((groups, rows, width), BF16),
            pltpu.VMEM((groups, rows, width), BF16),
            pltpu.VMEM((groups, rows, width), BF16),
            pltpu.VMEM((groups, per, cap, width), BF16),
            pltpu.VMEM((planes, cap, width), BF16),
            pltpu.VMEM((8, 128), F32),
            pltpu.VMEM((n, 8, 128), F32),
            dma((5,)), dma((3,)), dma((10,)), dma((1,)),
            dma((arrivals(n, ways_of_tokens(tok_rows))[1] if wide else 1,)),
            dma((max(1, narrow),)), dma((few, n if wide else 1)),
            dma((gathered, arrivals(n, ways_of(pieces, 0))[1])), dma((groups,)),
            dma((groups, arrivals(n, [False, True])[1])), dma((groups,)), dma((max(1, planes - 1),)), dma((1,)),
        ],
        compiler_params=pltpu.CompilerParams(
            collective_id=0, has_side_effects=True, vmem_limit_bytes=60 * 1024 * 1024
        ),
    )(
        tokens, norm_gain.reshape(1, width), routing.T, route_weight.T,
        gate_weight, up_weight, down_weight, final_gain.reshape(1, width),
    )


def solution(mesh):
    placed = (
        P("ep", "tp"),
        P("tp"),
        P("ep", None),
        P("ep", None),
        P("ep", None, "tp"),
        P("ep", None, "tp"),
        P("ep", None, "tp"),
        P("tp"),
    )
    return jax.shard_map(
        shards, mesh=mesh, in_specs=placed, out_specs=P("ep", "tp"), check_vma=False
    )
```

time: 68 us -> 62.9 us (0.925)
  Pallas kernels: 67.2 us -> 62 us
    pallas_call x1, Pallas kernels: 67.2 us -> 62 us  [shards(): pl.pallas_call(functools.partial(kernel, n, planes, groups, wide), out_sh...]
where the time goes in v2:
time: 62.9 us; the launch traced here: 62.7 us
  Pallas kernels  62 us (99%)
  local copies, waits for them, and re-layouts  0.66 us (1%)
    pallas_call x1, Pallas kernels, shards(): pl.pallas_call(functools.partial(kernel, n, planes, groups, wide), out_sh...  62 us

profile of v2, /device:TPU:0, one launch (start us, length us, event | category | flops | bytes accessed | tf_op | source)
XLA Modules:
  0.0 62.7 jit_solution(9955284857847332438)
XLA Ops:
  0.0 62.0 %shard_map.82 = bf16[128,512]{1,0:T(8,128)(2,1)S(1)} custom-call(bf16[128,512]{1,0:T(8,128)(2,1)} %tokens_hbm.1, f32[1,512]{1,0:T(1,128)} %bitcast.4, s32[2,128]{1,0:T(2,128)} %bitcast.6, f32[2,128]{1,0:T(2,128)} %bitcast.7, bf16[1,2048,896]{2,1,0:T(8,128)(2,1)} %gate_hbm.1, bf16[1,2048,896]{2,1,0:T(8,128)(2,1)} %up_hbm.1, bf16[1,3584,512]{2,1,0:T(8,128)(2,1)} %down_hbm.1, ...), custom_call_target="tpu_custom_call" | custom-call | tf_op jit(solution)/shard_map/pallas_call | solution.py:451
  62.1 0.7 %copy.10 = bf16[128,512]{1,0:T(8,128)(2,1)} copy(bf16[128,512]{1,0:T(8,128)(2,1)S(1)} %shard_map.82) | data formatting | bytes 262144
